TPU v7x, 32 devices: a whole 2x2x4 slice. The times are simulated.
32 devices in a mesh: sp: 8 (over z, x), tp: 4 (over y, core).
Axes of the slice: x: 2, y: 2, z: 4, core: 2. Of those that a mesh axis runs over, the one named last changes fastest.
Arguments:
- stream: bfloat16 [4096, 2048], P('sp', 'tp'), may hold values from -6 to 6
- norm_gain: float32 [2, 2048], replicated, may hold values from 0.1 to 1.9
- w_value: bfloat16 [2, 2048, 2048], P(None, 'sp', 'tp'), may hold values from -0.125 to 0.125
- w_inner: bfloat16 [2, 2048, 2048], P(None, 'sp', 'tp'), may hold values from -0.125 to 0.125
- w_outer: bfloat16 [2, 2048, 2048], P(None, 'sp', 'tp'), may hold values from -0.125 to 0.125
- conv_taps: float32 [2, 3, 2048], P(None, None, 'tp'), may hold values from -3 to 3
- w_output: bfloat16 [2, 2048, 2048], P(None, 'tp', 'sp'), may hold values from -0.125 to 0.125
Outputs:
- result: bfloat16 [4096, 2048], P('sp', 'tp')
All inputs are finite; a program needn't handle non-finite values.
Results may differ from a plain program's by a relative error of at most 0.02.
Values may be sent and summed in bfloat16 or wider, within the bound.
A program may use at most 64 MiB of HBM per device.

v0:
```python
import functools

import jax
import jax.numpy as jnp
from jax import lax
from jax.experimental import pallas as pl
from jax.experimental.pallas import tpu as pltpu
from jax.sharding import PartitionSpec as P

EPSILON = 1e-06
MESH = pl.DeviceIdType.MESH
F32 = jnp.float32
BF16 = jnp.bfloat16


def kernel(
    dims, stream, gain, w_value, w_inner, w_outer, taps, w_output, out,
    win, wout, held, normed, mix, outer, gated, tsend, s1, r1, r2a, r2b, t3a, t3b,
    r3a, r3b, tail, halo, send_sems, w_recv, swap_recv, local_sems, ag_recv, rs_recv,
):
    L, SP, TP, D, T, kb, nb, cb = dims
    Z = SP // 2
    half = T // 2
    sp, tp = lax.axis_index("sp"), lax.axis_index("tp")
    z, x = sp // 2, lax.rem(sp, 2)
    y, c = tp // 2, lax.rem(tp, 2)
    x_dev = (sp + 1 - 2 * x, tp)
    y_dev = (sp, tp + 2 - 4 * y)
    c_dev = (sp, tp + 1 - 2 * c)
    up_dev = (sp + 2, tp)
    down_dev = (sp - 2, tp)
    has_up, has_down = z < Z - 1, z > 0

    first = (2 * z >= Z).astype(jnp.int32)
    sends = []

    def make(src, dst, recv, dev):
        slot = len(sends)
        copy = lambda: pltpu.make_async_remote_copy(
            src_ref=src(), dst_ref=dst(), send_sem=send_sems.at[slot], recv_sem=recv(),
            device_id=dev, device_id_type=MESH)
        return copy

    def send(src, dst, recv, dev):
        copy = make(lambda: src, lambda: dst, lambda: recv, dev)
        sends.append((None, copy))
        copy().start()
        return copy

    def await_recv(ref, sem, dev=x_dev):
        pltpu.make_async_remote_copy(
            src_ref=ref, dst_ref=ref, send_sem=send_sems.at[0], recv_sem=sem,
            device_id=dev, device_id_type=MESH).wait_recv()

    w_in = (w_value, w_inner, w_outer)
    col = lambda q: pl.ds(pl.multiple_of(q * nb, nb), nb)
    krow = lambda s: pl.ds(pl.multiple_of(s * kb, kb), kb)

    def parts(l, s):
        return (win.at[l, :, krow(s), :], wout.at[l, s])

    def swap_parts(l, q, s):
        for i in range(3):
            yield i, w_in[i].at[l, :, col(q)], win.at[l, i, krow(s), :]
        yield 3, w_output.at[l, col(q), :], wout.at[l, s]

    def local_copies(l):
        return [pltpu.make_async_copy(src, dst, local_sems.at[l, i])
                for i, src, dst in swap_parts(l, x, sp)]

    def swap_start(l):
        for i, src, dst in swap_parts(l, 1 - x, sp):
            send(src, dst, swap_recv.at[l, i], x_dev)

    def swap_wait(l, part):
        for i, src, dst in swap_parts(l, x, x_dev[0]):
            if (i == 3) == (part == OUT):
                await_recv(dst, swap_recv.at[l, i])

    middle = jnp.logical_and(has_up, has_down)
    ends = jnp.logical_not(middle)
    IN, OUT = 0, 1

    def relay(l, part, h, picks=None, only=None):
        for p in (picks or (x, 1 - x)):
            for sign, neighbour, dev in ((-1, has_up, up_dev), (1, has_down, down_dev)):
                origin = z + sign * h
                cond = jnp.logical_and(neighbour, jnp.logical_and(origin >= 0, origin < Z))
                if only is not None:
                    cond = jnp.logical_and(cond, only)
                s = 2 * origin + p

                def copy(s=s, dev=dev, slot=len(sends)):
                    ref = parts(l, s)[part]
                    return pltpu.make_async_remote_copy(
                        src_ref=ref, dst_ref=ref, send_sem=send_sems.at[slot],
                        recv_sem=w_recv.at[l, s, part], device_id=dev, device_id_type=MESH)
                sends.append((cond, copy))

                @pl.when(cond)
                def _(s=s, copy=copy, dev=dev):
                    if h > 0:
                        await_recv(parts(l, s)[part], w_recv.at[l, s, part], dev)
                    copy().start()

    def weights_done(l, part, near=None):
        for d in range(1, Z):
            for sign, neighbour in ((-1, has_up), (1, has_down)):
                origin = z + sign * d
                inside = jnp.logical_and(origin >= 0, origin < Z)
                if near is not None:
                    same = (2 * origin >= Z) == (first == 1)
                    inside = jnp.logical_and(inside, same if near else jnp.logical_not(same))

                @pl.when(jnp.logical_and(jnp.logical_not(neighbour), inside))
                def _(origin=origin):
                    for p in range(2):
                        s = 2 * origin + p
                        await_recv(parts(l, s)[part], w_recv.at[l, s, part])

    rows_of = {0: pl.ds(0, half), 1: pl.ds(half, half)}

    def gather_start(l):
        for hf, dev in ((1, x_dev), (0, y_dev), (0, x_dev), (1, y_dev)):
            ref = held.at[l, tp, x, rows_of[hf], :]
            send(ref, ref, ag_recv.at[l, tp, x, hf], dev)
        ref = held.at[l, tp, x]
        send(ref, ref, ag_recv.at[l, tp, x, 0], c_dev)

    def gather_rest(l):
        ox, oy = 1 - x, y_dev[1]

        def got(j, xx, hf):
            await_recv(held.at[l, j, xx, rows_of[hf], :], ag_recv.at[l, j, xx, hf])

        got(tp, ox, 1)
        ref = held.at[l, tp, ox, rows_of[1], :]
        send(ref, ref, ag_recv.at[l, tp, ox, 1], y_dev)
        got(oy, x, 0)
        ref = held.at[l, oy, x, rows_of[0], :]
        send(ref, ref, ag_recv.at[l, oy, x, 0], x_dev)
        for j, xx, waits in ((tp, ox, (0,)), (oy, x, (1,)), (oy, ox, (0, 1))):
            for hf in waits:
                got(j, xx, hf)
            ref = held.at[l, j, xx]
            send(ref, ref, ag_recv.at[l, j, xx, 0], c_dev)
        cj, coy = c_dev[1], c_dev[1] + 2 - 4 * y
        for j in (cj, coy):
            for xx in range(2):
                await_recv(held.at[l, j, xx], ag_recv.at[l, j, xx, 0])

    nr = min(128, T)
    per = T // nr

    def normalize(l):
        def body(i, carry):
            xx, r = i // per, lax.rem(i, per)
            rows = pl.ds(pl.multiple_of(r * nr, nr), nr)
            blocks = [held[l, j, xx, rows, :].astype(F32) for j in range(TP)]
            total = sum(jnp.sum(b * b, axis=-1, keepdims=True) for b in blocks)
            scale = lax.rsqrt(total * (1.0 / D) + EPSILON)
            to = pl.ds(pl.multiple_of(i * nr, nr), nr)
            for j in range(TP):
                g = gain[l:l + 1, j * cb:(j + 1) * cb]
                normed[to, j * cb:(j + 1) * cb] = (blocks[j] * scale * g).astype(BF16)
            return carry
        lax.fori_loop(0, 2 * per, body, 0)

    pb = T
    mb = min(256, T)
    mper = T // mb

    def project(l):
        def body(i, carry):
            rows = pl.ds(pl.multiple_of(i * pb, pb), pb)
            n = normed[rows, :]
            v = jnp.dot(n, win[l, 0], preferred_element_type=F32)
            g = jnp.dot(n, win[l, 1], preferred_element_type=F32)
            mix[pl.ds(pl.multiple_of(16 + i * pb, 16), pb), :] = (g * v).astype(BF16).astype(F32)
            outer[rows, :] = jnp.dot(n, win[l, 2], preferred_element_type=F32)
            return carry
        lax.fori_loop(0, 2, body, 0)
        tail[l] = mix[2 * T:2 * T + 16, :].astype(BF16)
        copy = make(lambda: tail.at[l], lambda: halo.at[l], lambda: rs_recv.at[l, 0], up_dev)
        sends.append((has_up, copy))

        @pl.when(has_up)
        def _():
            copy().start()

    def w_block(l, j):
        per_tp = SP // TP
        return jnp.concatenate([wout[l, j * per_tp + q] for q in range(per_tp)], axis=1)

    def convolve(l):
        mix[0:16, :] = jnp.zeros((16, nb), F32)

        @pl.when(has_down)
        def _():
            await_recv(halo.at[l], rs_recv.at[l, 0])
            mix[0:16, :] = halo[l].astype(F32)

        tap = taps[l, :, col(x)]

        def body(i, carry):
            m = mix[pl.ds(pl.multiple_of(8 + i * mb, 8), mb + 8), :]
            conv = tap[0:1] * m[6:6 + mb] + tap[1:2] * m[7:7 + mb] + tap[2:3] * m[8:8 + mb]
            rows = pl.ds(pl.multiple_of(i * mb, mb), mb)
            gated[rows, :] = (outer[rows, :] * conv).astype(BF16)
            return carry
        lax.fori_loop(0, 2 * mper, body, 0)

    def outputs(l, yj, target, core, finish):
        w = w_block(l, 2 * yj + core)

        def body(i, carry):
            g = gated[pl.ds(pl.multiple_of(i * pb, pb), pb), :]
            t = jnp.dot(g, w, preferred_element_type=F32).astype(BF16)
            if finish:
                t = (t.astype(F32) + r1[l, yj, i].astype(F32)).astype(BF16)
            target[l, yj, i] = t
            return carry
        if finish:
            await_recv(r1.at[l, yj], rs_recv.at[l, 1 + yj])
        lax.fori_loop(0, 2, body, 0)
        if not finish:
            send(tsend.at[l, yj], r1.at[l, yj], rs_recv.at[l, 1 + yj], c_dev)

    def output_group(l, yj):
        A, B = rows_of[0], rows_of[1]
        outputs(l, yj, tsend, 1 - c, False)
        outputs(l, yj, s1, c, True)
        send(s1.at[l, yj, 1 - x, A, :], r2a.at[l, yj], rs_recv.at[l, 3 + yj], x_dev)
        other = yj != y
        for xj in (1 - x, x):
            copy = make(
                lambda xj=xj: s1.at[l, yj, xj, B, :], lambda xj=xj: r2b.at[l, xj],
                lambda xj=xj: rs_recv.at[l, 5 + xj], y_dev)
            sends.append((other, copy))

            @pl.when(other)
            def _(copy=copy):
                copy().start()

    def f(ref):
        return ref.astype(F32)

    def reduce(l, store):
        A, B = rows_of[0], rows_of[1]
        await_recv(r2a.at[l, 1 - y], rs_recv.at[l, 4 - y])
        t3a[l] = (f(s1[l, 1 - y, x, A, :]) + f(r2a[l, 1 - y])).astype(BF16)
        send(t3a.at[l], r3a.at[l], rs_recv.at[l, 7], y_dev)
        await_recv(r2b.at[l, 1 - x], rs_recv.at[l, 6 - x])
        t3b[l] = (f(s1[l, y, 1 - x, B, :]) + f(r2b[l, 1 - x])).astype(BF16)
        send(t3b.at[l], r3b.at[l], rs_recv.at[l, 8], x_dev)
        await_recv(r2a.at[l, y], rs_recv.at[l, 3 + y])
        await_recv(r3a.at[l], rs_recv.at[l, 7])
        branch = f(s1[l, y, x, A, :]) + f(r2a[l, y]) + f(r3a[l])
        store(A, (f(held[l, tp, x, A, :]) + branch).astype(BF16))
        await_recv(r2b.at[l, x], rs_recv.at[l, 5 + x])
        await_recv(r3b.at[l], rs_recv.at[l, 8])
        branch = f(s1[l, y, x, B, :]) + f(r2b[l, x]) + f(r3b[l])
        store(B, (f(held[l, tp, x, B, :]) + branch).astype(BF16))

    copies = [local_copies(l) for l in range(L)]
    for group in copies:
        for copy in group:
            copy.start()
    held[0, tp, x] = stream[...]

    barrier = pltpu.get_barrier_semaphore()
    for dev in (x_dev, y_dev, c_dev):
        pl.semaphore_signal(barrier, inc=1, device_id=dev, device_id_type=MESH)
    for cond, dev in ((has_up, up_dev), (has_down, down_dev)):
        @pl.when(cond)
        def _(dev=dev):
            pl.semaphore_signal(barrier, inc=1, device_id=dev, device_id_type=MESH)
    peers = 3 + has_up.astype(jnp.int32) + has_down.astype(jnp.int32)
    pl.semaphore_wait(barrier, peers)

    swap_start(0)
    for copy in copies[0][:3]:
        copy.wait()
    relay(0, IN, 0, (x,))
    copies[0][3].wait()
    relay(0, OUT, 0, (x,))
    gather_start(0)
    swap_wait(0, IN)
    relay(0, IN, 0, (1 - x,))
    swap_wait(0, OUT)
    relay(0, OUT, 0, (1 - x,), only=ends)
    if Z > 2:
        relay(0, IN, 1)
    gather_rest(0)
    for l in range(1, L):
        swap_start(l)
    for h in range(2, Z - 1):
        relay(0, IN, h)
    relay(0, OUT, 0, (1 - x,), only=middle)
    normalize(0)
    for l in range(1, L):
        for copy in copies[l]:
            copy.wait()
        swap_wait(l, IN)
        swap_wait(l, OUT)
        relay(l, IN, 0, only=ends)
        relay(l, OUT, 0, only=ends)
    for l in range(L):
        weights_done(l, IN)
        project(l)
        for h in range(1, Z - 1):
            relay(l, OUT, h)
        if l + 1 < L:
            relay(l + 1, IN, 0, only=middle)
        convolve(l)
        weights_done(l, OUT, True)
        output_group(l, first)
        weights_done(l, OUT, False)
        output_group(l, 1 - first)
        if l + 1 < L:
            def store(rows, value, l=l):
                held[l + 1, tp, x, rows, :] = value
            if Z > 2:
                relay(l + 1, IN, 1)
            reduce(l, store)
            gather_start(l + 1)
            for h in range(2, Z - 1):
                relay(l + 1, IN, h)
            gather_rest(l + 1)
            relay(l + 1, OUT, 0, only=middle)
            normalize(l + 1)
        else:
            def store(rows, value):
                out[rows, :] = value
            reduce(l, store)

    for cond, copy in sends:
        if cond is None:
            copy().wait_send()
        else:
            @pl.when(cond)
            def _(copy=copy):
                copy().wait_send()


def on_device(SP, TP, stream, norm_gain, w_value, w_inner, w_outer, conv_taps, w_output):
    L, kb, cb = w_value.shape
    T, D = stream.shape[0], norm_gain.shape[1]
    nb, Z = cb // 2, SP // 2
    dims = (L, SP, TP, D, T, kb, nb, cb)
    vmem = pl.BlockSpec(memory_space=pltpu.VMEM)
    hbm = pl.BlockSpec(memory_space=pl.ANY)
    half = T // 2
    n_sends = L * (4 + 8 * max(Z - 1, 1) + 8 + 10 + 13)
    return pl.pallas_call(
        functools.partial(kernel, dims),
        out_shape=jax.ShapeDtypeStruct((T, cb), BF16),
        in_specs=[vmem, vmem, hbm, hbm, hbm, vmem, hbm],
        out_specs=vmem,
        scratch_shapes=[
            pltpu.VMEM((L, 3, D, nb), BF16),
            pltpu.VMEM((L, SP, nb, kb), BF16),
            pltpu.VMEM((L, TP, 2, T, cb), BF16),
            pltpu.VMEM((2 * T, D), BF16),
            pltpu.VMEM((2 * T + 16, nb), F32),
            pltpu.VMEM((2 * T, nb), F32),
            pltpu.VMEM((2 * T, nb), BF16),
            pltpu.VMEM((L, 2, 2, T, cb), BF16),
            pltpu.VMEM((L, 2, 2, T, cb), BF16),
            pltpu.VMEM((L, 2, 2, T, cb), BF16),
            pltpu.VMEM((L, 2, half, cb), BF16),
            pltpu.VMEM((L, 2, half, cb), BF16),
            pltpu.VMEM((L, half, cb), BF16),
            pltpu.VMEM((L, half, cb), BF16),
            pltpu.VMEM((L, half, cb), BF16),
            pltpu.VMEM((L, half, cb), BF16),
            pltpu.VMEM((L, 16, nb), BF16),
            pltpu.VMEM((L, 16, nb), BF16),
            pltpu.SemaphoreType.DMA((n_sends,)),
            pltpu.SemaphoreType.DMA((L, SP, 2)),
            pltpu.SemaphoreType.DMA((L, 4)),
            pltpu.SemaphoreType.DMA((L, 4)),
            pltpu.SemaphoreType.DMA((L, TP, 2, 2)),
            pltpu.SemaphoreType.DMA((L, 9)),
        ],
        compiler_params=pltpu.CompilerParams(
            collective_id=0, has_side_effects=True, vmem_limit_bytes=60 * 1024 * 1024
        ),
    )(stream, norm_gain, w_value, w_inner, w_outer, conv_taps, w_output)


def solution(mesh):
    SP, TP = mesh.shape["sp"], mesh.shape["tp"]
    in_specs = (
        P("sp", "tp"),
        P(),
        P(None, "sp", "tp"),
        P(None, "sp", "tp"),
        P(None, "sp", "tp"),
        P(None, None, "tp"),
        P(None, "tp", "sp"),
    )
    return jax.shard_map(
        functools.partial(on_device, SP, TP),
        mesh=mesh, in_specs=in_specs, out_specs=P("sp", "tp"), check_vma=False,
    )
```

profile of v0, /device:TPU:0, one launch (start us, length us, event | category | flops | bytes accessed | tf_op | source)
XLA Modules:
  0.0 165.5 jit_solution(2036277818208213517)
XLA Ops:
  0.0 1.3 copy.8.taps
  1.3 162.3 %shard_map.73 = bf16[512,512]{1,0:T(8,128)(2,1)} custom-call(bf16[512,512]{1,0:T(8,128)(2,1)} %stream.1, f32[2,2048]{1,0:T(2,128)} %gain.1, bf16[2,256,512]{2,1,0:T(8,128)(2,1)} %w_value.1, bf16[2,256,512]{2,1,0:T(8,128)(2,1)} %w_inner.1, bf16[2,256,512]{2,1,0:T(8,128)(2,1)} %w_outer.1, f32[2,3,512]{2,1,0:T(4,128)} %copy.8.taps, bf16[2,512,256]{2,1,0:T(8,128)(2,1)} %w_output.1), custom_call_target="tpu_custom_call" | custom-call | tf_op jit(solution)/shard_map/pallas_call | solution.py:355
  163.7 1.9 %copy.10 = bf16[512,512]{1,0:T(8,128)(2,1)} copy(bf16[512,512]{1,0:T(8,128)(2,1)} %shard_map.73) | data formatting | bytes 1048576
where the time goes:
time: 168 us; the launch traced here: 166 us
  Pallas kernels  162 us (96%)
  local copies, waits for them, and re-layouts  3.18 us (2%)
    pallas_call x1, Pallas kernels, on_device(): pl.pallas_call(functools.partial(kernel, dims), out_shape=jax.ShapeDtypeS...  162 us

commit v1 on v0

v1 whole, which is shorter than its diff:
```python
import functools

import jax
import jax.numpy as jnp
from jax import lax
from jax.experimental import pallas as pl
from jax.experimental.pallas import tpu as pltpu
from jax.sharding import PartitionSpec as P

EPSILON = 1e-06
MESH = pl.DeviceIdType.MESH
F32 = jnp.float32
BF16 = jnp.bfloat16
HALO = 16


def kernel(
    dims, stream, gain, w_value, w_inner, w_outer, taps, w_output, out,
    win, wout, held, normed, mix, outer, gated, tsend, r1, s1, ra, s2, rb, tail, halo,
    send_sems, own_sems, fwd_sems, relay_sems, w_recv, local_sems, ag_recv, r1_recv,
    ra_recv, rb_recv, halo_recv,
):
    L, SP, TP, D, T, kb, nb, cb = dims
    Z = SP // 2
    half = T // 2
    sp, tp = lax.axis_index("sp"), lax.axis_index("tp")
    z, x = sp // 2, lax.rem(sp, 2)
    q = lax.rem(z, 2)
    y, c = tp // 2, lax.rem(tp, 2)
    x_dev = (sp + 1 - 2 * x, tp)
    y_dev = (sp, tp + 2 - 4 * y)
    c_dev = (sp, tp + 1 - 2 * c)
    pair_dev = (sp + 2 - 4 * q, tp)
    side_dev = (sp - 2 + 4 * q, tp)
    up_dev = (sp + 4, tp)
    down_dev = (sp - 4, tp)
    has_side = jnp.where(q == 0, z, Z - 1 - z) > 0
    has_up, has_down = z + 2 < Z, z >= 2
    tail_out = jnp.logical_and(x == 1, has_up)
    tail_in = jnp.logical_and(x == 0, has_down)
    at_end = jnp.logical_not(has_side)

    sends = []

    def start_if(cond, copy):
        sends.append((cond, copy))
        if cond is None:
            copy().start()
        else:
            @pl.when(cond)
            def _():
                copy().start()

    def remote(src, dst, send_sem, recv_sem, dev):
        return pltpu.make_async_remote_copy(
            src_ref=src, dst_ref=dst, send_sem=send_sem, recv_sem=recv_sem,
            device_id=dev, device_id_type=MESH)

    slots = [0]

    def send(src, dst, recv, dev, cond=None):
        slot = slots[0]
        slots[0] += 1
        start_if(cond, lambda: remote(src, dst, send_sems.at[slot], recv, dev))

    def await_recv(ref, sem):
        remote(ref, ref, send_sems.at[0], sem, x_dev).wait_recv()

    w_in = (w_value, w_inner, w_outer)
    KINDS = 4
    col = lambda p: pl.ds(pl.multiple_of(p * nb, nb), nb)
    krow = lambda s: pl.ds(pl.multiple_of(s * kb, kb), kb)

    def source(l, i, p):
        if i < 3:
            return w_in[i].at[l, :, col(p)]
        return w_output.at[l, col(p), :]

    def part(l, s, i):
        if i < 3:
            return win.at[l, i, krow(s), :]
        return wout.at[l, s]

    def local_copy(l, i):
        return pltpu.make_async_copy(source(l, i, q), part(l, sp, i), local_sems.at[l, i])

    def own_x(l, i):
        start_if(None, lambda: remote(
            source(l, i, q), part(l, sp, i), fwd_sems.at[l, z, i], w_recv.at[l, sp, i], x_dev))

    def own_to(l, i, k, cond, p, dev):
        start_if(cond, lambda: remote(
            source(l, i, p), part(l, sp, i), own_sems.at[l, i, k], w_recv.at[l, sp, i], dev))

    def own_pair(l, i, cond=None):
        own_to(l, i, 0, cond, 1 - q, pair_dev)

    def own_rest(l, i):
        own_to(l, i, 1, has_side, 1 - q, side_dev)
        own_to(l, i, 2, has_up, q, up_dev)
        own_to(l, i, 3, has_down, q, down_dev)

    def take(l, d, i):
        for sign, has_onward, onward in ((-1, has_up, up_dev), (1, has_down, down_dev)):
            origin = z + sign * d
            cond = jnp.logical_and(origin >= 0, origin < Z)
            s = 2 * origin + x

            def forward(s=s, origin=origin):
                ref = part(l, s, i)
                return remote(ref, ref, fwd_sems.at[l, origin, i], w_recv.at[l, s, i], x_dev)

            def relay(s=s, origin=origin, onward=onward):
                ref = part(l, s, i)
                return remote(ref, ref, relay_sems.at[l, origin, i], w_recv.at[l, s, i], onward)

            both = jnp.logical_and(cond, has_onward)
            sends.append((cond, forward))
            sends.append((both, relay))

            @pl.when(cond)
            def _(s=s, forward=forward, relay=relay, has_onward=has_onward):
                await_recv(part(l, s, i), w_recv.at[l, s, i])

                @pl.when(has_onward)
                def _():
                    relay().start()
                forward().start()

    lag = lambda d: (d - 1) // 2
    n_steps = KINDS + lag(Z - 1)

    def take_step(l, k):
        for d in range(1, Z):
            i = k - lag(d)
            if 0 <= i < KINDS:
                take(l, d, i)

    def weights_ready(l, i):
        local_copy(l, i).wait()
        for o in range(Z):
            s = 2 * o + 1 - x
            await_recv(part(l, s, i), w_recv.at[l, s, i])

    rows_of = (pl.ds(0, half), pl.ds(half, half))
    ty, tc, tyc = y_dev[1], c_dev[1], c_dev[1] + 2 - 4 * y

    def spread(l, b, j, h, dev):
        ref = held.at[l, b, j, rows_of[h], :]
        send(ref, ref, ag_recv.at[l, b, j, h], dev)

    def got(l, b, j, h):
        await_recv(held.at[l, b, j, rows_of[h], :], ag_recv.at[l, b, j, h])

    def gather_pair(l, h):
        got(l, 1 - q, tp, h)
        spread(l, 1 - q, tp, h, y_dev)
        spread(l, 1 - q, tp, h, c_dev)

    def gather_y(l, b, h):
        got(l, b, ty, h)
        spread(l, b, ty, h, c_dev)

    def gather_core(l, b):
        for j in (tc, tyc):
            for h in range(2):
                got(l, b, j, h)

    nr = min(128, T)
    per = T // nr

    def normalize(l, b):
        def body(r, carry):
            rows = pl.ds(pl.multiple_of(r * nr, nr), nr)
            blocks = [held[l, b, j, rows, :].astype(F32) for j in range(TP)]
            total = sum(jnp.sum(v * v, axis=-1, keepdims=True) for v in blocks)
            scale = lax.rsqrt(total * (1.0 / D) + EPSILON)
            to = pl.ds(pl.multiple_of(b * T + r * nr, nr), nr)
            for j in range(TP):
                g = gain[l:l + 1, j * cb:(j + 1) * cb]
                normed[to, j * cb:(j + 1) * cb] = (blocks[j] * scale * g).astype(BF16)
            return carry
        lax.fori_loop(0, per, body, 0)

    mb = min(256, T)
    mper = T // mb
    block = lambda b: pl.ds(pl.multiple_of(b * T, T), T)

    def project_mix(l, b):
        n = normed[block(b), :]
        v = jnp.dot(n, win[l, 0], preferred_element_type=F32)
        g = jnp.dot(n, win[l, 1], preferred_element_type=F32)
        m = (g * v).astype(BF16)
        mix[b, HALO:, :] = m.astype(F32)
        tail[l, b] = m[T - HALO:, :]

    def project_outer(l, b):
        n = normed[block(b), :]
        outer[block(b), :] = jnp.dot(n, win[l, 2], preferred_element_type=F32)

    def send_tail(l, b):
        near = jnp.logical_or(x == 0, b == 0)
        far = jnp.logical_and(tail_out, b == 1)
        src, to = tail.at[l, b], jnp.minimum(b + x, 1)
        send(src, halo.at[l, to], halo_recv.at[l, to], x_dev, near)
        send(src, halo.at[l, 0], halo_recv.at[l, 0], (sp + 3, tp), far)

    def convolve(l, b):
        first = jnp.logical_and(jnp.logical_and(x == 0, b == 0), jnp.logical_not(has_down))
        mix[b, 0:HALO, :] = jnp.zeros((HALO, nb), F32)

        @pl.when(jnp.logical_not(first))
        def _():
            await_recv(halo.at[l, b], halo_recv.at[l, b])
            mix[b, 0:HALO, :] = halo[l, b].astype(F32)

        tap = taps[l, :, col(q)]
        o = HALO - 8

        def body(i, carry):
            m = mix[b, pl.ds(pl.multiple_of(o + i * mb, 8), mb + 8), :]
            conv = tap[0:1] * m[6:6 + mb] + tap[1:2] * m[7:7 + mb] + tap[2:3] * m[8:8 + mb]
            rows = pl.ds(pl.multiple_of(b * T + i * mb, mb), mb)
            gated[rows, :] = (outer[rows, :] * conv).astype(BF16)
            return carry
        lax.fori_loop(0, mper, body, 0)

    per_tp = SP // TP

    def w_block(l, j):
        return jnp.concatenate([wout[l, j * per_tp + p] for p in range(per_tp)], axis=1)

    def product(l, b, yj, core):
        return jnp.dot(gated[block(b), :], w_block(l, 2 * yj + core),
                       preferred_element_type=F32).astype(BF16)

    def f(ref):
        return ref.astype(F32)

    order = ((1 - q, 1 - y), (q, 1 - y), (1 - q, y), (q, y))

    def y_first(l, h):
        return l + 1 < L or h == 0

    def outputs(l):
        for b, yj in order:
            tsend[l, b, yj] = product(l, b, yj, 1 - c)
            send(tsend.at[l, b, yj], r1.at[l, b, yj], r1_recv.at[l, b, yj], c_dev)
        for k, (b, yj) in enumerate(order):
            t = product(l, b, yj, c)
            await_recv(r1.at[l, b, yj], r1_recv.at[l, b, yj])
            s1[l, b, yj] = (f(t) + f(r1[l, b, yj])).astype(BF16)
            for h in range(2):
                rows = rows_of[h]
                if y_first(l, h) and k in (0, 1):
                    at, dev = b, y_dev
                elif not y_first(l, h) and k in (0, 2):
                    at, dev = yj, pair_dev
                else:
                    continue
                send(s1.at[l, b, yj, rows, :], ra.at[l, at, rows, :], ra_recv.at[l, at, h], dev)

    def reduce_second(l, h):
        rows = rows_of[h]
        if y_first(l, h):
            at, mine, dev = 1 - q, (1 - q, y), pair_dev
        else:
            at, mine, dev = 1 - y, (q, 1 - y), y_dev
        await_recv(ra.at[l, at, rows, :], ra_recv.at[l, at, h])
        s2[l, rows, :] = (f(s1[l, mine[0], mine[1], rows, :]) + f(ra[l, at, rows, :])).astype(BF16)
        send(s2.at[l, rows, :], rb.at[l, rows, :], rb_recv.at[l, h], dev)

    def reduce_last(l, h):
        rows = rows_of[h]
        at = q if y_first(l, h) else y
        await_recv(ra.at[l, at, rows, :], ra_recv.at[l, at, h])
        await_recv(rb.at[l, rows, :], rb_recv.at[l, h])
        branch = f(s1[l, q, y, rows, :]) + f(ra[l, at, rows, :]) + f(rb[l, rows, :])
        return (f(held[l, q, tp, rows, :]) + branch).astype(BF16)

    def compute(l):
        for b in (q, 1 - q):
            project_mix(l, b)
            send_tail(l, b)
            if b is q:
                weights_ready(l, 2)
            project_outer(l, b)
        turn = jnp.where(x == 1, q, 1 - q)
        convolve(l, turn)
        convolve(l, 1 - turn)

    for l in range(L):
        for i in range(KINDS):
            local_copy(l, i).start()
    held[0, q, tp] = stream[...]

    barrier = pltpu.get_barrier_semaphore()
    count = 4
    for dev in (x_dev, y_dev, c_dev, pair_dev):
        pl.semaphore_signal(barrier, inc=1, device_id=dev, device_id_type=MESH)
    for cond, dev in ((has_side, side_dev), (has_up, up_dev), (has_down, down_dev)):
        count = count + cond.astype(jnp.int32)

        @pl.when(cond)
        def _(dev=dev):
            pl.semaphore_signal(barrier, inc=1, device_id=dev, device_id_type=MESH)

    @pl.when(tail_in)
    def _():
        pl.semaphore_signal(barrier, inc=1, device_id=(sp - 3, tp), device_id_type=MESH)
    pl.semaphore_wait(barrier, count + tail_out.astype(jnp.int32))

    for i in range(KINDS):
        own_x(0, i)
        own_pair(0, i)
        own_rest(0, i)
        if i == 0:
            for h in range(2):
                spread(0, q, tp, h, pair_dev)
                spread(0, q, tp, h, y_dev)
                spread(0, q, tp, h, c_dev)
    for l in range(1, L):
        for i in range(KINDS):
            own_pair(l, i, at_end)

    def gather_rest_start(l):
        for h in range(2):
            gather_pair(l, h)
            gather_y(l, q, h)

    def own_next(l, i):
        own_x(l, i)
        own_rest(l, i)

    not_end = has_side
    for l in range(L):
        more = l + 1 < L
        if l == 0:
            take_step(0, 0)
            take_step(0, 1)
            gather_rest_start(0)
            take_step(0, 2)
            gather_core(0, q)
            normalize(0, q)
            for h in range(2):
                gather_y(0, 1 - q, h)
            for k in range(3, n_steps):
                take_step(0, k)
            gather_core(0, 1 - q)
            normalize(0, 1 - q)
        else:
            gather_core(l, q)
            normalize(l, q)
            for h in range(2):
                gather_y(l, 1 - q, h)
            for k in range(3, n_steps):
                take_step(l, k)
            gather_core(l, 1 - q)
            normalize(l, 1 - q)
        if more:
            for i in range(KINDS):
                own_next(l + 1, i)
            for i in range(2):
                own_pair(l + 1, i, not_end)
        weights_ready(l, 0)
        weights_ready(l, 1)
        compute(l)
        weights_ready(l, 3)
        outputs(l)
        if more:
            take_step(l + 1, 0)
            for h in range(2):
                reduce_second(l, h)
            for i in range(2, KINDS):
                own_pair(l + 1, i, not_end)
            take_step(l + 1, 1)
            for h in range(2):
                held[l + 1, q, tp, rows_of[h], :] = reduce_last(l, h)
                spread(l + 1, q, tp, h, y_dev)
                spread(l + 1, q, tp, h, pair_dev)
                spread(l + 1, q, tp, h, c_dev)
            take_step(l + 1, 2)
            gather_rest_start(l + 1)
        else:
            for h in range(2):
                reduce_second(l, h)
            for h in range(2):
                out[rows_of[h], :] = reduce_last(l, h)

    for cond, copy in sends:
        if cond is None:
            copy().wait_send()
        else:
            @pl.when(cond)
            def _(copy=copy):
                copy().wait_send()


def on_device(SP, TP, stream, norm_gain, w_value, w_inner, w_outer, conv_taps, w_output):
    L, kb, cb = w_value.shape
    T, D = stream.shape[0], norm_gain.shape[1]
    nb, Z = cb // 2, SP // 2
    dims = (L, SP, TP, D, T, kb, nb, cb)
    vmem = pl.BlockSpec(memory_space=pltpu.VMEM)
    hbm = pl.BlockSpec(memory_space=pl.ANY)
    dma = pltpu.SemaphoreType.DMA
    n_sends = L * 28
    return pl.pallas_call(
        functools.partial(kernel, dims),
        out_shape=jax.ShapeDtypeStruct((T, cb), BF16),
        in_specs=[vmem, vmem, hbm, hbm, hbm, vmem, hbm],
        out_specs=vmem,
        scratch_shapes=[
            pltpu.VMEM((L, 3, D, nb), BF16),
            pltpu.VMEM((L, SP, nb, kb), BF16),
            pltpu.VMEM((L, 2, TP, T, cb), BF16),
            pltpu.VMEM((2 * T, D), BF16),
            pltpu.VMEM((2, T + HALO, nb), F32),
            pltpu.VMEM((2 * T, nb), F32),
            pltpu.VMEM((2 * T, nb), BF16),
            pltpu.VMEM((L, 2, 2, T, cb), BF16),
            pltpu.VMEM((L, 2, 2, T, cb), BF16),
            pltpu.VMEM((L, 2, 2, T, cb), BF16),
            pltpu.VMEM((L, 2, T, cb), BF16),
            pltpu.VMEM((L, T, cb), BF16),
            pltpu.VMEM((L, T, cb), BF16),
            pltpu.VMEM((L, 2, HALO, nb), BF16),
            pltpu.VMEM((L, 2, HALO, nb), BF16),
            dma((n_sends,)),
            dma((L, 4, 4)),
            dma((L, Z, 4)),
            dma((L, Z, 4)),
            dma((L, SP, 4)),
            dma((L, 4)),
            dma((L, 2, TP, 2)),
            dma((L, 2, 2)),
            dma((L, 2, 2)),
            dma((L, 2)),
            dma((L, 2)),
        ],
        compiler_params=pltpu.CompilerParams(
            collective_id=0, has_side_effects=True, vmem_limit_bytes=60 * 1024 * 1024
        ),
    )(stream, norm_gain, w_value, w_inner, w_outer, conv_taps, w_output)


def solution(mesh):
    SP, TP = mesh.shape["sp"], mesh.shape["tp"]
    in_specs = (
        P("sp", "tp"),
        P(),
        P(None, "sp", "tp"),
        P(None, "sp", "tp"),
        P(None, "sp", "tp"),
        P(None, None, "tp"),
        P(None, "tp", "sp"),
    )
    return jax.shard_map(
        functools.partial(on_device, SP, TP),
        mesh=mesh, in_specs=in_specs, out_specs=P("sp", "tp"), check_vma=False,
    )
```

time: 168 us -> 181 us (1.077)
  the two profiles are of different devices: /device:TPU:0 before, /device:TPU:17 now
where the time goes in v1:
time: 181 us
  Pallas kernels  178 us (98%)
  local copies, waits for them, and re-layouts  3.18 us (2%)
    pallas_call x1, Pallas kernels, on_device(): pl.pallas_call(functools.partial(kernel, dims), out_shape=jax.ShapeDtypeS...  178 us

profile of v1, /device:TPU:17, one launch (start us, length us, event | category | flops | bytes accessed | tf_op | source)
XLA Modules:
  0.0 181.1 jit_solution(5559333602180390199)
XLA Ops:
  0.0 1.3 copy.8.taps
  1.3 178.0 %shard_map.73 = bf16[512,512]{1,0:T(8,128)(2,1)} custom-call(bf16[512,512]{1,0:T(8,128)(2,1)} %stream.1, f32[2,2048]{1,0:T(2,128)} %gain.1, bf16[2,256,512]{2,1,0:T(8,128)(2,1)} %w_value.1, bf16[2,256,512]{2,1,0:T(8,128)(2,1)} %w_inner.1, bf16[2,256,512]{2,1,0:T(8,128)(2,1)} %w_outer.1, f32[2,3,512]{2,1,0:T(4,128)} %copy.8.taps, bf16[2,512,256]{2,1,0:T(8,128)(2,1)} %w_output.1), custom_call_target="tpu_custom_call" | custom-call | tf_op jit(solution)/shard_map/pallas_call | solution.py:408
  179.3 1.9 %copy.10 = bf16[512,512]{1,0:T(8,128)(2,1)} copy(bf16[512,512]{1,0:T(8,128)(2,1)} %shard_map.73) | data formatting | bytes 1048576

commit v2 on v1

--- a/solution.py
+++ b/solution.py
@@ -31,14 +31,11 @@
     y_dev = (sp, tp + 2 - 4 * y)
     c_dev = (sp, tp + 1 - 2 * c)
     pair_dev = (sp + 2 - 4 * q, tp)
-    side_dev = (sp - 2 + 4 * q, tp)
     up_dev = (sp + 4, tp)
     down_dev = (sp - 4, tp)
-    has_side = jnp.where(q == 0, z, Z - 1 - z) > 0
     has_up, has_down = z + 2 < Z, z >= 2
     tail_out = jnp.logical_and(x == 1, has_up)
     tail_in = jnp.logical_and(x == 0, has_down)
-    at_end = jnp.logical_not(has_side)
 
     sends = []
 
@@ -92,18 +89,28 @@
         start_if(cond, lambda: remote(
             source(l, i, p), part(l, sp, i), own_sems.at[l, i, k], w_recv.at[l, sp, i], dev))
 
-    def own_pair(l, i, cond=None):
-        own_to(l, i, 0, cond, 1 - q, pair_dev)
-
-    def own_rest(l, i):
-        own_to(l, i, 1, has_side, 1 - q, side_dev)
-        own_to(l, i, 2, has_up, q, up_dev)
-        own_to(l, i, 3, has_down, q, down_dev)
+    def inside(o):
+        return jnp.logical_and(o >= 0, o < Z)
+
+    reach = lambda l: min(3 if l == 0 else 2, Z - 1)
+    ahead = 1 - 2 * q
+
+    def own_z(l, i, way, base):
+        for d in range(1, reach(l) + 1):
+            step = way * d
+            own_to(l, i, base + d - 1, inside(z + step), q if d % 2 == 0 else 1 - q,
+                   (sp + 2 * step, tp))
+
+    def toward(l, i):
+        own_z(l, i, ahead, 0)
+
+    def away(l, i):
+        own_z(l, i, -ahead, 3)
 
     def take(l, d, i):
         for sign, has_onward, onward in ((-1, has_up, up_dev), (1, has_down, down_dev)):
             origin = z + sign * d
-            cond = jnp.logical_and(origin >= 0, origin < Z)
+            cond = inside(origin)
             s = 2 * origin + x
 
             def forward(s=s, origin=origin):
@@ -114,27 +121,30 @@
                 ref = part(l, s, i)
                 return remote(ref, ref, relay_sems.at[l, origin, i], w_recv.at[l, s, i], onward)
 
-            both = jnp.logical_and(cond, has_onward)
+            relayed = reach(l) <= d + 1 and d + 2 < Z
             sends.append((cond, forward))
-            sends.append((both, relay))
+            if relayed:
+                sends.append((jnp.logical_and(cond, has_onward), relay))
 
             @pl.when(cond)
             def _(s=s, forward=forward, relay=relay, has_onward=has_onward):
                 await_recv(part(l, s, i), w_recv.at[l, s, i])
-
-                @pl.when(has_onward)
-                def _():
-                    relay().start()
+                if relayed:
+                    @pl.when(has_onward)
+                    def _():
+                        relay().start()
                 forward().start()
 
-    lag = lambda d: (d - 1) // 2
-    n_steps = KINDS + lag(Z - 1)
+    def hop(l, d):
+        return 0 if d <= reach(l) else 1 + (d - reach(l) - 1) // 2
+
+    def n_steps(l):
+        return KINDS * (1 + hop(l, Z - 1))
 
     def take_step(l, k):
         for d in range(1, Z):
-            i = k - lag(d)
-            if 0 <= i < KINDS:
-                take(l, d, i)
+            if hop(l, d) == k // KINDS:
+                take(l, d, k % KINDS)
 
     def weights_ready(l, i):
         local_copy(l, i).wait()
@@ -278,17 +288,6 @@
         branch = f(s1[l, q, y, rows, :]) + f(ra[l, at, rows, :]) + f(rb[l, rows, :])
         return (f(held[l, q, tp, rows, :]) + branch).astype(BF16)
 
-    def compute(l):
-        for b in (q, 1 - q):
-            project_mix(l, b)
-            send_tail(l, b)
-            if b is q:
-                weights_ready(l, 2)
-            project_outer(l, b)
-        turn = jnp.where(x == 1, q, 1 - q)
-        convolve(l, turn)
-        convolve(l, 1 - turn)
-
     for l in range(L):
         for i in range(KINDS):
             local_copy(l, i).start()
@@ -298,7 +297,11 @@
     count = 4
     for dev in (x_dev, y_dev, c_dev, pair_dev):
         pl.semaphore_signal(barrier, inc=1, device_id=dev, device_id_type=MESH)
-    for cond, dev in ((has_side, side_dev), (has_up, up_dev), (has_down, down_dev)):
+    others = [(inside(z - ahead), (sp - 2 * ahead, tp))]
+    for d in range(2, reach(0) + 1):
+        for way in (-1, 1):
+            others.append((inside(z + way * d), (sp + 2 * way * d, tp)))
+    for cond, dev in others:
         count = count + cond.astype(jnp.int32)
 
         @pl.when(cond)
@@ -310,82 +313,116 @@
         pl.semaphore_signal(barrier, inc=1, device_id=(sp - 3, tp), device_id_type=MESH)
     pl.semaphore_wait(barrier, count + tail_out.astype(jnp.int32))
 
-    for i in range(KINDS):
-        own_x(0, i)
-        own_pair(0, i)
-        own_rest(0, i)
-        if i == 0:
-            for h in range(2):
-                spread(0, q, tp, h, pair_dev)
-                spread(0, q, tp, h, y_dev)
-                spread(0, q, tp, h, c_dev)
-    for l in range(1, L):
-        for i in range(KINDS):
-            own_pair(l, i, at_end)
-
-    def gather_rest_start(l):
+    def gather_first(l):
         for h in range(2):
             gather_pair(l, h)
             gather_y(l, q, h)
 
-    def own_next(l, i):
-        own_x(l, i)
-        own_rest(l, i)
-
-    not_end = has_side
+    def gather_last(l):
+        for h in range(2):
+            gather_y(l, 1 - q, h)
+
+    def project(l, b):
+        project_mix(l, b)
+        send_tail(l, b)
+
+    def finish(l):
+        turn = jnp.where(x == 1, q, 1 - q)
+        convolve(l, turn)
+        convolve(l, 1 - turn)
+        weights_ready(l, 3)
+        outputs(l)
+
+    def advance(l, store):
+        def step(k):
+            if l + 1 < L and k < n_steps(l + 1):
+                take_step(l + 1, k)
+        step(0)
+        step(1)
+        reduce_second(l, 0)
+        step(2)
+        reduce_second(l, 1)
+        step(3)
+        step(4)
+        step(5)
+        store(0, reduce_last(l, 0))
+        step(6)
+        store(1, reduce_last(l, 1))
+        step(7)
+
+    for i in range(KINDS):
+        own_x(0, i)
+        toward(0, i)
+        away(0, i)
+        if i == 0:
+            for h in range(2):
+                spread(0, q, tp, h, y_dev)
+                spread(0, q, tp, h, c_dev)
+        if i < 2:
+            spread(0, q, tp, i, pair_dev)
     for l in range(L):
         more = l + 1 < L
         if l == 0:
             take_step(0, 0)
+            gather_y(0, q, 0)
+            gather_y(0, q, 1)
+            gather_pair(0, 0)
             take_step(0, 1)
-            gather_rest_start(0)
-            take_step(0, 2)
+            gather_pair(0, 1)
             gather_core(0, q)
             normalize(0, q)
-            for h in range(2):
-                gather_y(0, 1 - q, h)
-            for k in range(3, n_steps):
-                take_step(0, k)
+            take_step(0, 2)
+            gather_last(0)
             gather_core(0, 1 - q)
             normalize(0, 1 - q)
+            weights_ready(0, 0)
+            weights_ready(0, 1)
+            project(0, q)
+            project(0, 1 - q)
+            if more:
+                for i in range(KINDS):
+                    toward(1, i)
+                    away(1, i)
+            for k in range(3, n_steps(l)):
+                take_step(0, k)
+            if more:
+                for i in range(KINDS):
+                    own_x(1, i)
+            weights_ready(0, 2)
+            project_outer(0, q)
+            project_outer(0, 1 - q)
         else:
+            gather_first(l)
+            for k in range(8, n_steps(l)):
+                take_step(l, k)
             gather_core(l, q)
             normalize(l, q)
-            for h in range(2):
-                gather_y(l, 1 - q, h)
-            for k in range(3, n_steps):
-                take_step(l, k)
+            if more:
+                for i in range(KINDS):
+                    toward(l + 1, i)
+                    away(l + 1, i)
+                    own_x(l + 1, i)
+            for i in range(3):
+                weights_ready(l, i)
+            project(l, q)
+            project_outer(l, q)
+            gather_last(l)
             gather_core(l, 1 - q)
             normalize(l, 1 - q)
+            project(l, 1 - q)
+            project_outer(l, 1 - q)
+        finish(l)
         if more:
-            for i in range(KINDS):
-                own_next(l + 1, i)
-            for i in range(2):
-                own_pair(l + 1, i, not_end)
-        weights_ready(l, 0)
-        weights_ready(l, 1)
-        compute(l)
-        weights_ready(l, 3)
-        outputs(l)
-        if more:
-            take_step(l + 1, 0)
-            for h in range(2):
-                reduce_second(l, h)
-            for i in range(2, KINDS):
-                own_pair(l + 1, i, not_end)
-            take_step(l + 1, 1)
-            for h in range(2):
-                held[l + 1, q, tp, rows_of[h], :] = reduce_last(l, h)
+            def store(h, value, l=l):
+                held[l + 1, q, tp, rows_of[h], :] = value
                 spread(l + 1, q, tp, h, y_dev)
                 spread(l + 1, q, tp, h, pair_dev)
                 spread(l + 1, q, tp, h, c_dev)
-            take_step(l + 1, 2)
-            gather_rest_start(l + 1)
+            advance(l, store)
         else:
-            for h in range(2):
-                reduce_second(l, h)
-            for h in range(2):
-                out[rows_of[h], :] = reduce_last(l, h)
+            def store(h, value):
+                out[rows_of[h], :] = value
+            advance(l, store)
 
     for cond, copy in sends:
         if cond is None:
@@ -427,7 +464,7 @@
             pltpu.VMEM((L, 2, HALO, nb), BF16),
             pltpu.VMEM((L, 2, HALO, nb), BF16),
             dma((n_sends,)),
-            dma((L, 4, 4)),
+            dma((L, 4, 6)),
             dma((L, Z, 4)),
             dma((L, Z, 4)),
             dma((L, SP, 4)),

time: 181 us -> 153 us (0.85)
  the two profiles are of different devices: /device:TPU:17 before, /device:TPU:0 now
where the time goes in v2:
time: 153 us
  Pallas kernels  150 us (98%)
  local copies, waits for them, and re-layouts  3.18 us (2%)
    pallas_call x1, Pallas kernels, on_device(): pl.pallas_call(functools.partial(kernel, dims), out_shape=jax.ShapeDtypeS...  150 us
    unnamed x2, local copies, waits for them, and re-layouts  3.18 us

profile of v2, /device:TPU:0, one launch (start us, length us, event | category | flops | bytes accessed | tf_op | source)
XLA Modules:
  0.0 153.2 jit_solution(12905714584278906900)
XLA Ops:
  0.0 1.3 copy.8.taps
  1.3 150.0 %shard_map.73 = bf16[512,512]{1,0:T(8,128)(2,1)} custom-call(bf16[512,512]{1,0:T(8,128)(2,1)} %stream.1, f32[2,2048]{1,0:T(2,128)} %gain.1, bf16[2,256,512]{2,1,0:T(8,128)(2,1)} %w_value.1, bf16[2,256,512]{2,1,0:T(8,128)(2,1)} %w_inner.1, bf16[2,256,512]{2,1,0:T(8,128)(2,1)} %w_outer.1, f32[2,3,512]{2,1,0:T(4,128)} %copy.8.taps, bf16[2,512,256]{2,1,0:T(8,128)(2,1)} %w_output.1), custom_call_target="tpu_custom_call" | custom-call | tf_op jit(solution)/shard_map/pallas_call | solution.py:445
  151.3 1.9 %copy.10 = bf16[512,512]{1,0:T(8,128)(2,1)} copy(bf16[512,512]{1,0:T(8,128)(2,1)} %shard_map.73) | data formatting | bytes 1048576

commit v3 on v2

v3 whole, which is shorter than its diff:
```python
import functools

import jax
import jax.numpy as jnp
from jax import lax
from jax.experimental import pallas as pl
from jax.experimental.pallas import tpu as pltpu
from jax.sharding import PartitionSpec as P

EPSILON = 1e-06
MESH = pl.DeviceIdType.MESH
F32 = jnp.float32
BF16 = jnp.bfloat16
HALO = 16
SPLIT = 2


def reach_of(l, k, Z):
    return min(3 if l == 0 or k >= 2 * SPLIT else 2, Z - 1)


def relayed_of(l, k, d, Z):
    return d + 2 < Z and d + 2 > reach_of(l, k, Z)


def relay_slots(L, Z):
    return [(l, d) for l in range(L) for d in range(1, Z)
            if any(relayed_of(l, k, d, Z) for k in range(4 * SPLIT))]


def kernel(
    dims, stream, gain, w_value, w_inner, w_outer, taps, w_output, out,
    win, wout, held, normed, mix, outer, gated, tsend, r1, s1, ra, s2, rb, tail, halo,
    send_sems, own_sems, fwd_sems, relay_sems, z_recv, x_recv, local_sems, ag_recv, core_recv,
    r1_recv, ra_recv, rb_recv, halo_recv,
):
    L, SP, TP, D, T, kb, nb, cb = dims
    Z = SP // 2
    half = T // 2
    sp, tp = lax.axis_index("sp"), lax.axis_index("tp")
    z, x = sp // 2, lax.rem(sp, 2)
    q = lax.rem(z, 2)
    y, c = tp // 2, lax.rem(tp, 2)
    x_dev = (sp + 1 - 2 * x, tp)
    y_dev = (sp, tp + 2 - 4 * y)
    c_dev = (sp, tp + 1 - 2 * c)
    pair_dev = (sp + 2 - 4 * q, tp)
    has_up, has_down = z + 2 < Z, z >= 2
    tail_out = jnp.logical_and(x == 1, has_up)
    tail_in = jnp.logical_and(x == 0, has_down)

    def start_if(cond, copy):
        if cond is None:
            copy().start()
        else:
            @pl.when(cond)
            def _():
                copy().start()

    def remote(src, dst, send_sem, recv_sem, dev):
        return pltpu.make_async_remote_copy(
            src_ref=src, dst_ref=dst, send_sem=send_sem, recv_sem=recv_sem,
            device_id=dev, device_id_type=MESH)

    RELAY, OWN, OWN_CORE, PARTIAL, FIRST, SECOND, TAIL = range(7)

    def send(slot, src, dst, recv, dev, l, cond=None):
        start_if(cond, lambda: remote(src, dst, send_sems.at[l, slot], recv, dev))

    def await_recv(ref, sem):
        remote(ref, ref, send_sems.at[0, 0], sem, x_dev).wait_recv()

    def await_send(ref, sem, cond=None):
        wait = lambda: remote(ref, ref, sem, x_recv.at[0, 0], x_dev).wait_send()
        if cond is None:
            wait()
        else:
            pl.when(cond)(wait)

    w_in = (w_value, w_inner, w_outer)
    KINDS = 4 * SPLIT
    kp, np_ = kb // SPLIT, nb // SPLIT
    col = lambda p: pl.ds(pl.multiple_of(p * nb, nb), nb)

    def source(l, k, p):
        i, r = k // SPLIT, k % SPLIT
        if i < 3:
            return w_in[i].at[l, pl.ds(r * kp, kp), col(p)]
        return w_output.at[l, pl.ds(pl.multiple_of(p * nb + r * np_, np_), np_), :]

    def part(l, s, k):
        i, r = k // SPLIT, k % SPLIT
        if i < 3:
            return win.at[l, i, pl.ds(pl.multiple_of(s * kb + r * kp, kp), kp), :]
        return wout.at[l, s, pl.ds(r * np_, np_), :]

    def local_copy(l, i):
        if i < 3:
            src, dst = w_in[i].at[l, :, col(q)], win.at[l, i, pl.ds(pl.multiple_of(sp * kb, kb), kb), :]
        else:
            src, dst = w_output.at[l, col(q), :], wout.at[l, sp]
        return pltpu.make_async_copy(src, dst, local_sems.at[l, i])

    def own_x(l, k):
        remote(source(l, k, q), part(l, sp, k), fwd_sems.at[l, z], x_recv.at[l, k // SPLIT],
               x_dev).start()

    def own_to(l, i, k, cond, p, dev):
        start_if(cond, lambda: remote(
            source(l, i, p), part(l, sp, i), own_sems.at[l, k], z_recv.at[l, z, i], dev))

    def inside(o):
        return jnp.logical_and(o >= 0, o < Z)

    reach = lambda l, i: reach_of(l, i, Z)
    ahead = 1 - 2 * q

    def own_z(l, i, way, base):
        for d in range(1, reach(l, i) + 1):
            step = way * d
            own_to(l, i, base + d - 1, inside(z + step), q if d % 2 == 0 else 1 - q,
                   (sp + 2 * step, tp))

    def toward(l, i):
        own_z(l, i, ahead, 0)

    def away(l, i):
        own_z(l, i, -ahead, 3)

    relays = relay_slots(L, Z)
    ways = (-ahead, ahead)

    def take(l, i, side, d, who=None):
        way = ways[side]
        origin = z + way * d
        cond = inside(origin)
        if who is not None:
            cond = jnp.logical_and(cond, who)
        s = 2 * origin + x
        ref = part(l, s, i)
        beyond = z - 2 * way
        relayed = relayed_of(l, i, d, Z)
        sem = z_recv.at[l, origin, i]

        @pl.when(cond)
        def _():
            await_recv(ref, sem)
            if relayed:
                @pl.when(inside(beyond))
                def _():
                    remote(ref, ref, relay_sems.at[relays.index((l, d)), side], sem,
                           (2 * beyond + x, tp)).start()
            remote(ref, ref, fwd_sems.at[l, origin], x_recv.at[l, i // SPLIT], x_dev).start()

    def take_pair(l, i, who=None):
        take(l, i, 1, 1, who)

    def take_others(l, i, who=None):
        take(l, i, 0, 1, who)
        for d in range(2, reach(l, i) + 1):
            take(l, i, 1, d, who)
            take(l, i, 0, d, who)

    def take_near(l, *ks):
        for k in ks:
            take_others(l, k)
            take_pair(l, k)

    def take_far(l, *ks):
        for k in ks:
            for d in range(reach(l, k) + 1, Z):
                take(l, k, 1, d)
                take(l, k, 0, d)

    def weights_ready(l, i):
        local_copy(l, i).wait()
        ref = win.at[l, i, pl.ds(0, Z * kb), :] if i < 3 else wout.at[l, pl.ds(0, Z)]
        await_recv(ref, x_recv.at[l, i])

    def pieces(*matrices):
        return [i * SPLIT + r for i in matrices for r in range(SPLIT)]

    def issue(l, *matrices):
        for k in pieces(*matrices):
            toward(l, k)
            away(l, k)

    rows_of = (pl.ds(0, half), pl.ds(half, half))
    ty = y_dev[1]

    FROM_PAIR, FROM_Y = 0, 1

    def spread(slot, l, b, h, to, cond=None):
        ref = held.at[l, b, tp, rows_of[h], :]
        send(slot, ref, ref, ag_recv.at[l, b, to, h], (pair_dev, y_dev)[to], l, cond)

    def to_core(slot, l, b, j, h):
        ref = held.at[l, b, j, rows_of[h], :]
        send(slot, ref, ref, core_recv.at[l, b], c_dev, l)

    def got(l, b, j, h, origin):
        await_recv(held.at[l, b, j, rows_of[h], :], ag_recv.at[l, b, origin, h])

    def spread_own(l, h):
        spread(OWN, l, q, h, FROM_Y)
        to_core(OWN_CORE, l, q, tp, h)

    def gather_pair(l, h):
        got(l, 1 - q, tp, h, FROM_PAIR)
        spread(RELAY, l, 1 - q, h, FROM_Y)
        to_core(RELAY, l, 1 - q, tp, h)

    def gather_y(l, b, h):
        got(l, b, ty, h, FROM_Y)
        to_core(RELAY, l, b, ty, h)

    def gather_core(l, b):
        await_recv(held.at[l, b, pl.ds(0, 2)], core_recv.at[l, b])

    nr = min(128, T)
    per = T // nr

    def normalize(l, b):
        def body(r, carry):
            rows = pl.ds(pl.multiple_of(r * nr, nr), nr)
            blocks = [held[l, b, j, rows, :].astype(F32) for j in range(TP)]
            total = sum(jnp.sum(v * v, axis=-1, keepdims=True) for v in blocks)
            scale = lax.rsqrt(total * (1.0 / D) + EPSILON)
            to = pl.ds(pl.multiple_of(b * T + r * nr, nr), nr)
            for j in range(TP):
                g = gain[l:l + 1, j * cb:(j + 1) * cb]
                normed[to, j * cb:(j + 1) * cb] = (blocks[j] * scale * g).astype(BF16)
            return carry
        lax.fori_loop(0, per, body, 0)

    mb = min(256, T)
    mper = T // mb
    block = lambda b: pl.ds(pl.multiple_of(b * T, T), T)

    def project_mix(l, b):
        n = normed[block(b), :]
        v = jnp.dot(n, win[l, 0], preferred_element_type=F32)
        g = jnp.dot(n, win[l, 1], preferred_element_type=F32)
        m = (g * v).astype(BF16)
        mix[b, HALO:, :] = m.astype(F32)
        tail[l, b] = m[T - HALO:, :]

    def project_outer(l, b):
        n = normed[block(b), :]
        outer[block(b), :] = jnp.dot(n, win[l, 2], preferred_element_type=F32)

    def send_tail(l, b, n):
        near = jnp.logical_or(x == 0, b == 0)
        far = jnp.logical_and(tail_out, b == 1)
        src, to = tail.at[l, b], jnp.minimum(b + x, 1)
        send(TAIL + n, src, halo.at[l, to], halo_recv.at[l, to], x_dev, l, near)
        send(TAIL + n, src, halo.at[l, 0], halo_recv.at[l, 0], (sp + 3, tp), l, far)

    def convolve(l, b):
        first = jnp.logical_and(jnp.logical_and(x == 0, b == 0), jnp.logical_not(has_down))
        mix[b, 0:HALO, :] = jnp.zeros((HALO, nb), F32)

        @pl.when(jnp.logical_not(first))
        def _():
            await_recv(halo.at[l, b], halo_recv.at[l, b])
            mix[b, 0:HALO, :] = halo[l, b].astype(F32)

        tap = taps[:, l, col(q)]
        o = HALO - 8

        def body(i, carry):
            m = mix[b, pl.ds(pl.multiple_of(o + i * mb, 8), mb + 8), :]
            conv = tap[0:1] * m[6:6 + mb] + tap[1:2] * m[7:7 + mb] + tap[2:3] * m[8:8 + mb]
            rows = pl.ds(pl.multiple_of(b * T + i * mb, mb), mb)
            gated[rows, :] = (outer[rows, :] * conv).astype(BF16)
            return carry
        lax.fori_loop(0, mper, body, 0)

    per_tp = SP // TP

    def w_block(l, j):
        return jnp.concatenate([wout[l, j * per_tp + p] for p in range(per_tp)], axis=1)

    def product(l, b, yj, core):
        return jnp.dot(gated[block(b), :], w_block(l, 2 * yj + core),
                       preferred_element_type=F32).astype(BF16)

    def f(ref):
        return ref.astype(F32)

    order = ((1 - q, 1 - y), (q, 1 - y), (1 - q, y), (q, y))

    def y_first(l, h):
        return l + 1 < L or h == 0

    def outputs(l):
        for b, yj in order:
            tsend[l, b, yj] = product(l, b, yj, 1 - c)
            send(PARTIAL, tsend.at[l, b, yj], r1.at[l, b, yj], r1_recv.at[l, b, yj], c_dev, l)
        for k, (b, yj) in enumerate(order):
            t = product(l, b, yj, c)
            await_recv(r1.at[l, b, yj], r1_recv.at[l, b, yj])
            s1[l, b, yj] = (f(t) + f(r1[l, b, yj])).astype(BF16)
            for h in range(2):
                rows = rows_of[h]
                if y_first(l, h) and k in (0, 1):
                    at, dev = b, y_dev
                elif not y_first(l, h) and k in (0, 2):
                    at, dev = yj, pair_dev
                else:
                    continue
                send(FIRST, s1.at[l, b, yj, rows, :], ra.at[l, at, rows, :],
                     ra_recv.at[l, at, h], dev, l)

    def reduce_second(l, h):
        rows = rows_of[h]
        if y_first(l, h):
            at, mine, dev = 1 - q, (1 - q, y), pair_dev
        else:
            at, mine, dev = 1 - y, (q, 1 - y), y_dev
        await_recv(ra.at[l, at, rows, :], ra_recv.at[l, at, h])
        s2[l, rows, :] = (f(s1[l, mine[0], mine[1], rows, :]) + f(ra[l, at, rows, :])).astype(BF16)
        send(SECOND, s2.at[l, rows, :], rb.at[l, rows, :], rb_recv.at[l, h], dev, l)

    def reduce_last(l, h):
        rows = rows_of[h]
        at = q if y_first(l, h) else y
        await_recv(ra.at[l, at, rows, :], ra_recv.at[l, at, h])
        await_recv(rb.at[l, rows, :], rb_recv.at[l, h])
        branch = f(s1[l, q, y, rows, :]) + f(ra[l, at, rows, :]) + f(rb[l, rows, :])
        return (f(held[l, q, tp, rows, :]) + branch).astype(BF16)

    for l in range(L):
        for i in range(4):
            local_copy(l, i).start()
    held[0, q, tp] = stream[...]

    barrier = pltpu.get_barrier_semaphore()
    count = 4
    for dev in (x_dev, y_dev, c_dev, pair_dev):
        pl.semaphore_signal(barrier, inc=1, device_id=dev, device_id_type=MESH)
    others = [(inside(z - ahead), (sp - 2 * ahead, tp))]
    for d in range(2, reach(0, 0) + 1):
        for way in (-1, 1):
            others.append((inside(z + way * d), (sp + 2 * way * d, tp)))
    for cond, dev in others:
        count = count + cond.astype(jnp.int32)

        @pl.when(cond)
        def _(dev=dev):
            pl.semaphore_signal(barrier, inc=1, device_id=dev, device_id_type=MESH)

    @pl.when(tail_in)
    def _():
        pl.semaphore_signal(barrier, inc=1, device_id=(sp - 3, tp), device_id_type=MESH)
    pl.semaphore_wait(barrier, count + tail_out.astype(jnp.int32))

    def gather_first(l):
        for h in range(2):
            gather_pair(l, h)
            gather_y(l, q, h)

    def gather_last(l):
        for h in range(2):
            gather_y(l, 1 - q, h)

    def project(l, b):
        project_mix(l, b)
        send_tail(l, b, 0 if b is q else 1)

    def finish(l):
        turn = jnp.where(x == 1, q, 1 - q)
        convolve(l, turn)
        convolve(l, 1 - turn)
        weights_ready(l, 3)
        outputs(l)

    def flush_weights(l):
        size = lambda n: win.at[l, 0, pl.ds(0, n * kp), :]
        for side in range(2):
            for d in range(1, Z):
                to = z + ways[side] * d
                n = sum(d <= reach(l, k) for k in range(KINDS))
                if n:
                    await_send(size(n), own_sems.at[l, 3 * (1 - side) + d - 1], inside(to))
                n = sum(relayed_of(l, k, d, Z) for k in range(KINDS))
                if n:
                    both = jnp.logical_and(inside(to), inside(z - 2 * ways[side]))
                    await_send(size(n), relay_sems.at[relays.index((l, d)), side], both)
        for o in range(Z):
            await_send(size(KINDS), fwd_sems.at[l, o])

    def flush_gather(l):
        await_send(held.at[l, 0], send_sems.at[l, RELAY])
        await_send(ra.at[l], send_sems.at[l, OWN])
        await_send(rb.at[l], send_sems.at[l, OWN_CORE])

    def flush_layer(l):
        await_send(tsend.at[l], send_sems.at[l, PARTIAL])
        await_send(ra.at[l], send_sems.at[l, FIRST])
        await_send(rb.at[l], send_sems.at[l, SECOND])
        for n, b in ((0, q), (1, 1 - q)):
            near = jnp.logical_or(x == 0, b == 0)
            far = jnp.logical_and(tail_out, b == 1)
            await_send(tail.at[l, 0], send_sems.at[l, TAIL + n], jnp.logical_or(near, far))

    def advance(l, store):
        n = l + 1
        if n == L:
            for h in range(2):
                reduce_second(l, h)
            for m in range(L):
                flush_weights(m)
                flush_gather(m)
                if m < l:
                    flush_layer(m)
            for h in range(2):
                store(h, reduce_last(l, h))
            return
        issue(n, 2)
        take_near(n, *pieces(0, 1))
        for h in range(2):
            reduce_second(l, h)
        take_far(n, *pieces(0))
        store(0, reduce_last(l, 0))
        take_far(n, *pieces(1))
        store(1, reduce_last(l, 1))
        take_near(n, *pieces(2))
        take_far(n, *pieces(2))

    inner = inside(z - ahead)
    outer_end = jnp.logical_not(inner)
    for h in range(2):
        spread_own(0, h)
    for k in range(KINDS):
        own_x(0, k)
        toward(0, k)
        away(0, k)
        if k == SPLIT - 1:
            spread(OWN, 0, q, 0, FROM_PAIR)
            spread(OWN, 0, q, 1, FROM_PAIR, inner)
        if k == 2 * SPLIT - 1:
            spread(OWN, 0, q, 1, FROM_PAIR, outer_end)

    def first_arrivals():
        for k in range(SPLIT):
            take_near(0, k)
        for h in range(2):
            gather_y(0, q, h)
        for k in range(SPLIT, 2 * SPLIT):
            take_others(0, k)
            take_pair(0, k, inner)
            if k == SPLIT:
                gather_pair(0, 0)
                gather_core(0, q)
                normalize(0, q)
        for k in pieces(2)[:1]:
            take_others(0, k, inner)
            take_pair(0, k, inner)
        gather_pair(0, 1)
        for k in pieces(2)[:1]:
            take_others(0, k, outer_end)
        for k in pieces(1) + pieces(2)[:1]:
            take_pair(0, k, outer_end)
        take_near(0, *pieces(2)[1:])
        gather_last(0)
        take_near(0, *pieces(3)[:-1])
        gather_core(0, 1 - q)
        normalize(0, 1 - q)
        weights_ready(0, 0)
        weights_ready(0, 1)
        project(0, q)
        take_near(0, *pieces(3)[-1:])
        take_far(0, *range(KINDS))
        project(0, 1 - q)

    for l in range(L):
        more = l + 1 < L
        if l == 0:
            first_arrivals()
            if more:
                issue(1, 0, 1)
                for k in range(KINDS):
                    own_x(1, k)
            weights_ready(0, 2)
            project_outer(0, q)
            project_outer(0, 1 - q)
        else:
            for h in range(2):
                gather_pair(l, h)
                gather_y(l, q, h)
                if h == 0:
                    issue(l, 3)
            gather_core(l, q)
            normalize(l, q)
            if more:
                issue(l + 1, 0, 1)
                for k in range(KINDS):
                    own_x(l + 1, k)
            for i in range(3):
                weights_ready(l, i)
            project(l, q)
            project_outer(l, q)
            take_near(l, *pieces(3))
            take_far(l, *pieces(3))
            gather_last(l)
            gather_core(l, 1 - q)
            normalize(l, 1 - q)
            project(l, 1 - q)
            project_outer(l, 1 - q)
        finish(l)
        if more:
            def store(h, value, l=l):
                held[l + 1, q, tp, rows_of[h], :] = value
                spread(OWN, l + 1, q, h, FROM_PAIR)
                spread_own(l + 1, h)
            advance(l, store)
        else:
            def store(h, value):
                out[rows_of[h], :] = value
            advance(l, store)

    flush_layer(L - 1)


def on_device(SP, TP, stream, norm_gain, w_value, w_inner, w_outer, conv_taps, w_output):
    L, kb, cb = w_value.shape
    T, D = stream.shape[0], norm_gain.shape[1]
    nb, Z = cb // 2, SP // 2
    dims = (L, SP, TP, D, T, kb, nb, cb)
    vmem = pl.BlockSpec(memory_space=pltpu.VMEM)
    hbm = pl.BlockSpec(memory_space=pl.ANY)
    dma = pltpu.SemaphoreType.DMA
    kinds = 4 * SPLIT
    n_relays = max(1, len(relay_slots(L, Z)))
    return pl.pallas_call(
        functools.partial(kernel, dims),
        out_shape=jax.ShapeDtypeStruct((T, cb), BF16),
        in_specs=[vmem, vmem, hbm, hbm, hbm, vmem, hbm],
        out_specs=vmem,
        scratch_shapes=[
            pltpu.VMEM((L, 3, D, nb), BF16),
            pltpu.VMEM((L, SP, nb, kb), BF16),
            pltpu.VMEM((L, 2, TP, T, cb), BF16),
            pltpu.VMEM((2 * T, D), BF16),
            pltpu.VMEM((2, T + HALO, nb), F32),
            pltpu.VMEM((2 * T, nb), F32),
            pltpu.VMEM((2 * T, nb), BF16),
            pltpu.VMEM((L, 2, 2, T, cb), BF16),
            pltpu.VMEM((L, 2, 2, T, cb), BF16),
            pltpu.VMEM((L, 2, 2, T, cb), BF16),
            pltpu.VMEM((L, 2, T, cb), BF16),
            pltpu.VMEM((L, T, cb), BF16),
            pltpu.VMEM((L, T, cb), BF16),
            pltpu.VMEM((L, 2, HALO, nb), BF16),
            pltpu.VMEM((L, 2, HALO, nb), BF16),
            dma((L, 8)),
            dma((L, 6)),
            dma((L, Z)),
            dma((n_relays, 2)),
            dma((L, Z, kinds)),
            dma((L, 4)),
            dma((L, 4)),
            dma((L, 2, 2, 2)),
            dma((L, 2)),
            dma((L, 2, 2)),
            dma((L, 2, 2)),
            dma((L, 2)),
            dma((L, 2)),
        ],
        compiler_params=pltpu.CompilerParams(
            collective_id=0, has_side_effects=True, vmem_limit_bytes=60 * 1024 * 1024
        ),
    )(stream, norm_gain, w_value, w_inner, w_outer, jnp.transpose(conv_taps, (1, 0, 2)), w_output)


def solution(mesh):
    SP, TP = mesh.shape["sp"], mesh.shape["tp"]
    in_specs = (
        P("sp", "tp"),
        P(),
        P(None, "sp", "tp"),
        P(None, "sp", "tp"),
        P(None, "sp", "tp"),
        P(None, None, "tp"),
        P(None, "tp", "sp"),
    )
    return jax.shard_map(
        functools.partial(on_device, SP, TP),
        mesh=mesh, in_specs=in_specs, out_specs=P("sp", "tp"), check_vma=False,
    )
```

time: 153 us -> 150 us (0.980)
  Pallas kernels: 150 us -> 148 us
    pallas_call x1, Pallas kernels: 150 us -> 148 us  [on_device(): pl.pallas_call(functools.partial(kernel, dims), out_shape=jax.ShapeDtypeS...]
    unnamed x2 -> x1, local copies, waits for them, and re-layouts: 3.18 us -> 1.87 us
where the time goes in v3:
time: 150 us
  Pallas kernels  148 us (99%)
  local copies, waits for them, and re-layouts  1.87 us (1%)
    pallas_call x1, Pallas kernels, on_device(): pl.pallas_call(functools.partial(kernel, dims), out_shape=jax.ShapeDtypeS...  148 us

profile of v3, /device:TPU:0, one launch (start us, length us, event | category | flops | bytes accessed | tf_op | source)
XLA Modules:
  0.0 149.8 jit_solution(16032678007834348082)
XLA Ops:
  0.0 147.9 %shard_map.73 = bf16[512,512]{1,0:T(8,128)(2,1)} custom-call(bf16[512,512]{1,0:T(8,128)(2,1)} %stream.1, f32[2,2048]{1,0:T(2,128)} %gain.1, bf16[2,256,512]{2,1,0:T(8,128)(2,1)} %w_value.1, bf16[2,256,512]{2,1,0:T(8,128)(2,1)} %w_inner.1, bf16[2,256,512]{2,1,0:T(8,128)(2,1)} %w_outer.1, f32[3,2,512]{2,1,0:T(2,128)} %bitcast.1, bf16[2,512,256]{2,1,0:T(8,128)(2,1)} %w_output.1), custom_call_target="tpu_custom_call" | custom-call | tf_op jit(solution)/shard_map/pallas_call | solution.py:536
  147.9 1.9 %copy.9 = bf16[512,512]{1,0:T(8,128)(2,1)} copy(bf16[512,512]{1,0:T(8,128)(2,1)} %shard_map.73) | data formatting | bytes 1048576

commit v4 on v3

--- a/solution.py
+++ b/solution.py
@@ -417,14 +417,16 @@
             for h in range(2):
                 store(h, reduce_last(l, h))
             return
-        issue(n, 2)
-        take_near(n, *pieces(0, 1))
-        for h in range(2):
-            reduce_second(l, h)
+        if n > 1:
+            issue(n, 2)
+        take_near(n, *pieces(0))
+        reduce_second(l, 0)
+        take_near(n, *pieces(1))
+        reduce_second(l, 1)
+        store(0, reduce_last(l, 0))
         take_far(n, *pieces(0))
-        store(0, reduce_last(l, 0))
+        store(1, reduce_last(l, 1))
         take_far(n, *pieces(1))
-        store(1, reduce_last(l, 1))
         take_near(n, *pieces(2))
         take_far(n, *pieces(2))
 
@@ -479,7 +481,7 @@
         if l == 0:
             first_arrivals()
             if more:
-                issue(1, 0, 1)
+                issue(1, 0, 1, 2)
                 for k in range(KINDS):
                     own_x(1, k)
             weights_ready(0, 2)
@@ -487,8 +489,8 @@
             project_outer(0, 1 - q)
         else:
             for h in range(2):
+                gather_y(l, q, h)
                 gather_pair(l, h)
-                gather_y(l, q, h)
                 if h == 0:
                     issue(l, 3)
             gather_core(l, q)

time: 150 us -> 147 us (0.980)
  Pallas kernels: 148 us -> 145 us
    pallas_call x1, Pallas kernels: 148 us -> 145 us  [on_device(): pl.pallas_call(functools.partial(kernel, dims), out_shape=jax.ShapeDtypeS...]
where the time goes in v4:
time: 147 us
  Pallas kernels  145 us (99%)
  local copies, waits for them, and re-layouts  1.87 us (1%)
    pallas_call x1, Pallas kernels, on_device(): pl.pallas_call(functools.partial(kernel, dims), out_shape=jax.ShapeDtypeS...  145 us

profile of v4, /device:TPU:0, one launch (start us, length us, event | category | flops | bytes accessed | tf_op | source)
XLA Modules:
  0.0 146.8 jit_solution(10587317592763280045)
XLA Ops:
  0.0 144.9 %shard_map.73 = bf16[512,512]{1,0:T(8,128)(2,1)} custom-call(bf16[512,512]{1,0:T(8,128)(2,1)} %stream.1, f32[2,2048]{1,0:T(2,128)} %gain.1, bf16[2,256,512]{2,1,0:T(8,128)(2,1)} %w_value.1, bf16[2,256,512]{2,1,0:T(8,128)(2,1)} %w_inner.1, bf16[2,256,512]{2,1,0:T(8,128)(2,1)} %w_outer.1, f32[3,2,512]{2,1,0:T(2,128)} %bitcast.1, bf16[2,512,256]{2,1,0:T(8,128)(2,1)} %w_output.1), custom_call_target="tpu_custom_call" | custom-call | tf_op jit(solution)/shard_map/pallas_call | solution.py:538
  144.9 1.9 %copy.9 = bf16[512,512]{1,0:T(8,128)(2,1)} copy(bf16[512,512]{1,0:T(8,128)(2,1)} %shard_map.73) | data formatting | bytes 1048576
